TPU v7x, 512 devices: a whole 4x4x16 slice. The times are simulated.
512 devices in a mesh: sp: 64 (over z, y), tp: 8 (over x, core).
Axes of the slice: x: 4, y: 4, z: 16, core: 2. Of those that a mesh axis runs over, the one named last changes fastest.
Arguments:
- skip_stream_entering: bfloat16 [8192, 2048], P(('sp', 'tp')), may hold values from -6 to 6
- content_signal_matrix: bfloat16 [8192, 4096], P('sp', 'tp'), may hold values from -6 to 6
- writer_signal_matrix: bfloat16 [8192, 1024], P('sp', 'tp'), may hold values from -6 to 6
- reader_signal_matrix: bfloat16 [8192, 1024], P('sp', 'tp'), may hold values from -6 to 6
- multiplier_signal: bfloat16 [8192, 4096], P('sp', 'tp'), may hold values from -6 to 6
- interval_before_softplus: float32 [64, 8192], P('tp', 'sp'), may hold values from -7.5 to 0.5
- extra_log_shrink: float32 [64, 8192], P('tp', 'sp'), may hold values from -2.8 to 0
- log_forget_speed: float32 [64], P('tp'), may hold values from -12 to 0
- content_filter_coefs: bfloat16 [4, 4096], P(None, 'tp'), may hold values from -3 to 3
- writer_filter_coefs: bfloat16 [4, 1024], P(None, 'tp'), may hold values from -3 to 3
- reader_filter_coefs: bfloat16 [4, 1024], P(None, 'tp'), may hold values from -3 to 3
- skip_path_factor: float32 [64], P('tp'), may hold values from 0.25 to 2
- cluster_scaling_vector: float32 [4096], P('tp'), may hold values from 0.1 to 1.9
- blend_result_matrix: bfloat16 [4096, 2048], P('tp'), may hold values from -0.09375 to 0.09375
- feature_blend_scaling: float32 [2048], replicated, may hold values from 0.1 to 1.9
- widening_matrix: bfloat16 [2048, 8192], P('sp', 'tp'), may hold values from -0.125 to 0.125
- narrowing_matrix: bfloat16 [8192, 2048], P('tp', 'sp'), may hold values from -0.0625 to 0.0625
Outputs:
- layer_out: bfloat16 [8192, 2048], P(('sp', 'tp'))
All inputs are finite; a program needn't handle non-finite values.
Results may differ from a plain program's by a relative error of at most 0.02.
Values may be sent and summed in bfloat16 or wider, within the bound.
No kernel may reach another device: no remote copies, remote signals or barrier semaphores. Data moves between devices by JAX's collectives and lax.ppermute only.
A program may use at most 64 MiB of HBM per device.

v0:
```python
import jax
import jax.numpy as jnp
from jax import lax
from jax.sharding import Mesh
from jax.sharding import PartitionSpec as P

HEAD_DIM = 64
STATE = 128
BLOCK = 128
SP = ("sp_0", "sp_1")
SP_TP = ("sp_0", "sp_1", "tp")
epsilon = 1e-05


def turned_gather(arrays, axis, dims):
    turned = [jnp.moveaxis(a, dim, 0) for a, dim in zip(arrays, dims)]
    widths = [t[0].size for t in turned]
    both = jnp.concatenate([t.reshape(-1, w) for t, w in zip(turned, widths)], axis=1)
    out = lax.all_gather(both, axis, axis=0, tiled=True)
    blocks = jnp.split(out, [sum(widths[:k]) for k in range(1, len(widths))], axis=1)
    return tuple(
        (
            jnp.moveaxis(b.reshape(-1, *t.shape[1:]), 0, dim)
            for b, t, dim in zip(blocks, turned, dims)
        )
    )


def shifted(value, axis, steps):
    count = lax.axis_size(axis)
    initial, last = (max(0, -steps), min(count, count - steps))
    return lax.ppermute(value, axis, [(source, source + steps) for source in range(initial, last)])


def nothing_yet(value, identity):
    return jax.tree.map(
        lambda part, zero: jnp.zeros_like(part) + jnp.asarray(zero, part.dtype), value, identity
    )


def entering_2(value, axes, combine, identity):
    before = start = nothing_yet(value, identity)
    running = value
    for axis in reversed(axes):
        peers, mine = (lax.axis_size(axis), lax.axis_index(axis))
        pieces = jax.tree.map(
            lambda part, kind: lax.all_gather(part.astype(kind), axis),
            running,
            (jnp.bfloat16, jnp.bfloat16),
        )
        inside, running = (start, start)
        for k in range(peers):
            passed = k < mine
            running = combine(
                running, jax.tree.map(lambda part, own: part[k].astype(own.dtype), pieces, value)
            )
            inside = jax.tree.map(lambda new, old: jnp.where(passed, new, old), running, inside)
        before = combine(inside, before)
    return before


def in_blocks(value, dim, peers):
    dims = value.shape
    blocks = value.reshape(*dims[:dim], peers, dims[dim] // peers, *dims[dim + 1 :])
    return jnp.moveaxis(blocks, dim, 0)


def sum_at_owner(value, axis, dim):
    blocks = in_blocks(value, dim, lax.axis_size(axis))
    arrived = lax.all_to_all(blocks, axis, split_axis=0, concat_axis=0, tiled=True)
    return arrived.astype(jnp.float32).sum(axis=0)


def copy_for_each(value, axis):
    copies = jnp.broadcast_to(value, (lax.axis_size(axis), *value.shape))
    return lax.all_to_all(copies, axis, split_axis=0, concat_axis=0, tiled=True)


def laid_out(blocks, dim):
    dims = list(blocks.shape[1:])
    dims[dim] *= blocks.shape[0]
    return jnp.moveaxis(blocks, 0, dim).reshape(dims)


def gathered_copies(value, axis, dim):
    blocks = copy_for_each(value, axis)
    return laid_out(blocks, dim)


def convolve(inputs, rim_rows, conv_taps):
    width = conv_taps.shape[0]
    length = inputs.shape[0]
    extended = jnp.concatenate([rim_rows, inputs], axis=0)
    summed = extended[0:length].astype(jnp.float32) * conv_taps[0].astype(jnp.float32)
    for offset in range(1, width):
        summed = summed + extended[offset : offset + length].astype(jnp.float32) * conv_taps[
            offset
        ].astype(jnp.float32)
    return jax.nn.silu(summed)


def advance(carried, pair):
    block_state, block_factor = pair
    return (carried * block_factor[..., None, None] + block_state, carried)


def combine_states(earlier, following):
    return (earlier[0] * following[0], earlier[1] * following[0][..., None, None] + following[1])


def blockwise(values, interval_lengths, log_forgetting, key_rows, query_rows):
    length, groups, per_group, width = values.shape
    blocks = length // BLOCK
    value_blocks = values.reshape(blocks, BLOCK, groups, per_group, width)
    step_blocks = jnp.transpose(
        interval_lengths.reshape(groups, per_group, blocks, BLOCK), (2, 3, 0, 1)
    )
    weighted = value_blocks * step_blocks[..., None]
    cumulative = jnp.cumsum(
        jnp.transpose(log_forgetting.reshape(groups, per_group, blocks, BLOCK), (2, 0, 1, 3)),
        axis=-1,
    )
    key_blocks = key_rows.reshape(blocks, BLOCK, groups, -1)
    query_blocks = query_rows.reshape(blocks, BLOCK, groups, -1)
    causal = jnp.tril(jnp.ones((BLOCK, BLOCK), dtype=bool))
    decay_mask = jnp.exp(
        jnp.where(causal, cumulative[..., :, None] - cumulative[..., None, :], -jnp.inf)
    )
    scores = jnp.einsum("clgn,csgn->cgls", query_blocks, key_blocks)
    within = jnp.einsum("cgls,cgrls,csgrp->clgrp", scores, decay_mask, weighted)
    to_end = jnp.exp(cumulative[..., -1:] - cumulative)
    states = jnp.einsum("clgn,cgrl,clgrp->cgrpn", key_blocks, to_end, weighted)
    block_totals = cumulative[..., -1]
    initial = jnp.zeros(states.shape[1:], jnp.float32)
    final, entering = lax.scan(advance, initial, (states, jnp.exp(block_totals)))
    carried = jnp.einsum("clgn,cgrpn,cgrl->clgrp", query_blocks, entering, jnp.exp(cumulative))
    from_start = (jnp.cumsum(block_totals, axis=0) - block_totals)[..., None] + cumulative
    return (within + carried, final, from_start, jnp.sum(block_totals, axis=0))


def normalize(rows, gain):
    widened = rows.astype(jnp.float32)
    scaled = widened * lax.rsqrt(jnp.mean(widened * widened, axis=-1, keepdims=True) + epsilon)
    return (scaled * gain).astype(jnp.bfloat16)


def per_device(
    skip_stream_entering,
    content_signal_matrix,
    writer_signal_matrix,
    reader_signal_matrix,
    multiplier_signal,
    interval_before_softplus,
    extra_log_shrink,
    log_forget_speed,
    content_filter_coefs,
    writer_filter_coefs,
    reader_filter_coefs,
    skip_path_factor,
    cluster_scaling_vector,
    blend_result_matrix,
    feature_blend_scaling,
    widening_matrix,
    narrowing_matrix,
):
    up_whole, down_whole = turned_gather((widening_matrix, narrowing_matrix), SP, (0, 1))
    rim_width = content_filter_coefs.shape[0] - 1
    length = content_signal_matrix.shape[0]
    rims = shifted(
        (
            content_signal_matrix[length - rim_width :],
            writer_signal_matrix[length - rim_width :],
            reader_signal_matrix[length - rim_width :],
        ),
        SP,
        1,
    )
    values = convolve(content_signal_matrix, rims[0], content_filter_coefs)
    key_rows = convolve(writer_signal_matrix, rims[1], writer_filter_coefs)
    query_rows = convolve(reader_signal_matrix, rims[2], reader_filter_coefs)
    local_heads = interval_before_softplus.shape[0]
    local_groups = writer_signal_matrix.shape[1] // STATE
    per_group = local_heads // local_groups
    interval_lengths = jax.nn.softplus(interval_before_softplus)
    log_forgetting = extra_log_shrink - jnp.exp(log_forget_speed)[:, None] * interval_lengths
    shaped = values.reshape(length, local_groups, per_group, HEAD_DIM)
    local_out, end_state, from_start, device_total = blockwise(
        shaped,
        interval_lengths.reshape(local_groups, per_group, length),
        log_forgetting.reshape(local_groups, per_group, length),
        key_rows,
        query_rows,
    )
    identity = (jnp.ones_like(device_total), jnp.zeros_like(end_state))
    incoming = entering_2((jnp.exp(device_total), end_state), SP, combine_states, identity)[1]
    query_blocks = query_rows.reshape(length // BLOCK, BLOCK, local_groups, STATE)
    arriving = jnp.einsum("clgn,grpn,cgrl->clgrp", query_blocks, incoming, jnp.exp(from_start))
    scan_out = (local_out + arriving).reshape(length, local_heads * HEAD_DIM)
    gated = (scan_out + jnp.repeat(skip_path_factor, HEAD_DIM) * values) * jax.nn.silu(
        multiplier_signal.astype(jnp.float32)
    )
    grouped = gated.reshape(length, local_groups, -1)
    grouped = grouped * lax.rsqrt(jnp.mean(grouped * grouped, axis=-1, keepdims=True) + epsilon)
    heads_out = (grouped.reshape(length, -1) * cluster_scaling_vector).astype(jnp.bfloat16)
    mixer_rows = sum_at_owner(
        jnp.dot(heads_out, blend_result_matrix, preferred_element_type=jnp.float32).astype(
            jnp.bfloat16
        ),
        "tp",
        0,
    ).astype(jnp.bfloat16)
    own_rows = (skip_stream_entering.astype(jnp.float32) + mixer_rows.astype(jnp.float32)).astype(
        jnp.bfloat16
    )
    normed_all = gathered_copies(normalize(own_rows, feature_blend_scaling), "tp", 0)
    lifted = jnp.dot(normed_all, up_whole, preferred_element_type=jnp.float32)
    lifted = jax.nn.relu(lifted)
    hidden = (lifted * lifted).astype(jnp.bfloat16)
    mlp_rows = sum_at_owner(
        jnp.dot(hidden, down_whole, preferred_element_type=jnp.float32).astype(jnp.bfloat16),
        "tp",
        0,
    ).astype(jnp.bfloat16)
    return (own_rows.astype(jnp.float32) + mlp_rows.astype(jnp.float32)).astype(jnp.bfloat16)


def solution(mesh):
    torus = Mesh(mesh.devices.reshape(16, 4, mesh.shape["tp"]), ("sp_0", "sp_1", "tp"))
    placed = (
        P(SP_TP, None),
        P(SP, "tp"),
        P(SP, "tp"),
        P(SP, "tp"),
        P(SP, "tp"),
        P("tp", SP),
        P("tp", SP),
        P("tp"),
        P(None, "tp"),
        P(None, "tp"),
        P(None, "tp"),
        P("tp"),
        P("tp"),
        P("tp", None),
        P(),
        P(SP, "tp"),
        P("tp", SP),
    )
    return jax.shard_map(
        per_device, mesh=torus, in_specs=placed, out_specs=P(SP_TP, None), check_vma=False
    )
```

profile of v0, /device:TPU:1, one launch (start us, length us, event | category | flops | bytes accessed | tf_op | source)
XLA Modules:
  0.0 304.0 jit_solution(4290324773650001404)
XLA Ops:
  6.5 0.9 slice.212
  7.6 4.0 %collective-permute-start.2 = (bf16[3,512]{0,1:T(8,128)(2,1)S(1)}, bf16[3,512]{0,1:T(8,128)(2,1)S(1)}, u32[]{:S(2)}, u32[]{:S(2)}) collective-permute-start(bf16[3,512]{0,1:T(8,128)(2,1)S(1)} %copy.24), channel_id=1, source_target_pairs={{0,8},{8,16},{16,24},{24,32},{32,40},{40,48},{48,56},{56,64},{64,7... | collective-permute-start | bytes 9224 | tf_op jit(solution)/shard_map/ppermute | solution.py:32
  11.6 0.7 slice.204
  12.3 3.2 %collective-permute-start.1 = (bf16[3,128]{1,0:T(4,128)(2,1)S(1)}, bf16[3,128]{1,0:T(4,128)(2,1)S(1)}, u32[]{:S(2)}, u32[]{:S(2)}) collective-permute-start(bf16[3,128]{1,0:T(4,128)(2,1)S(1)} %slice.204), channel_id=1, source_target_pairs={{0,8},{8,16},{16,24},{24,32},{32,40},{40,48},{48,56},{56,64},{64,7... | collective-permute-start | bytes 2312 | tf_op jit(solution)/shard_map/ppermute | solution.py:32
  15.5 0.7 exp.73
  16.2 0.8 fusion.190
  17.5 0.9 slice_convert_fusion.3
  18.3 0.8 bitcast_convert_fusion.3
  19.3 8.0 %all-gather = bf16[4,1,8,1]{2,3,1,0:T(2,128)(2,1)S(1)} all-gather(bf16[1,1,8,1]{2,3,1,0:T(2,128)(2,1)S(1)} %copy.27), channel_id=2, replica_groups=mesh['sp_0'=16,'sp_1'=4,'tp'=8] {'sp_1'}, dimensions={0}, use_global_device_ids=true | all-gather | bytes 80 | tf_op jit(solution)/shard_map/all_gather | solution.py:47
  27.3 1.0 copy.25
  28.3 1.0 divide_multiply_fusion.1
  29.3 0.5 divide_multiply_fusion
  30.0 11.4 %all-gather.1 = bf16[32,64,128]{2,1,0:T(8,128)(2,1)S(1)} all-gather(bf16[8,64,128]{2,1,0:T(8,128)(2,1)S(1)} %fusion.22), channel_id=3, replica_groups=mesh['sp_0'=16,'sp_1'=4,'tp'=8] {'sp_1'}, dimensions={0}, use_global_device_ids=true | all-gather | bytes 655360 | tf_op jit(solution)/shard_map/all_gather | solution.py:47
  41.4 0.9 fusion.104
  42.4 1.6 pad_maximum_fusion.1
  43.9 0.7 slice.196
  44.6 1.3 collective-permute-start
  45.9 27.0 %all_gather.22 = bf16[16,1,8]{2,1,0:T(2,128)(2,1)S(1)} all-gather(bf16[1,1,8]{2,1,0:T(2,128)(2,1)S(1)} %convert_bitcast_fusion), channel_id=1, replica_groups=mesh['sp_0'=16,'sp_1'=4,'tp'=8] {'sp_0'}, dimensions={0}, use_global_device_ids=true | all-gather | bytes 272 | tf_op jit(solution)/shard_map/all_gather | solution.py:47
  73.0 0.8 bitcast_convert_fusion.7
  73.8 1.0 copy.28
  74.9 0.7 broadcast_in_dim.20
  75.7 1.0 divide_multiply_fusion.2
  77.0 34.8 %all-gather.5.cloned.1.call-done = bf16[16,1,8,64,128]{4,3,2,1,0:T(8,128)(2,1)} async-done(((bf16[1,1,8,64,128]{4,3,2,1,0:T(8,128)(2,1)}), bf16[16,1,8,64,128]{4,3,2,1,0:T(8,128)(2,1)}) %all-gather.5.cloned.1.call-update) | async-done | bytes 2097168 | tf_op jit(solution)/shard_map/all_gather | solution.py:47
  111.8 2.5 fusion.18
  114.4 0.4 fusion.21
  114.9 0.6 convolution_convert_fusion
  115.5 23.3 %all_to_all.15 = bf16[8,16,2048]{2,1,0:T(8,128)(2,1)S(1)} all-to-all(bf16[8,16,2048]{2,1,0:T(8,128)(2,1)S(1)} %bitcast.221), channel_id=1, replica_groups=mesh['sp_0'=16,'sp_1'=4,'tp'=8] {'tp'}, dimensions={0} | all-to-all | bytes 1048576 | tf_op jit(solution)/shard_map/all_to_all | solution.py:70
  139.2 12.8 %all_to_all.16 = bf16[8,16,2048]{2,1,0:T(8,128)(2,1)S(1)} all-to-all(bf16[8,16,2048]{2,1,0:T(8,128)(2,1)S(1)} %broadcast_in_dim.21), channel_id=1, replica_groups=mesh['sp_0'=16,'sp_1'=4,'tp'=8] {'tp'}, dimensions={0} | all-to-all | bytes 1048576 | tf_op jit(solution)/shard_map/all_to_all | solution.py:76
  151.9 117.2 %all-gather.7.cloned.1.call-done = bf16[2048,2048]{1,0:T(8,128)(2,1)} async-done(((bf16[32,2048]{1,0:T(8,128)(2,1)}), bf16[2048,2048]{1,0:T(8,128)(2,1)}) %all-gather.7.cloned.1.call-update) | async-done | bytes 8388624 | tf_op jit(solution)/shard_map/all_gather | solution.py:19
  269.1 5.6 %fusion.4 = bf16[128,2048]{1,0:T(8,128)(2,1)S(1)} fusion(bf16[2048,2048]{1,0:T(8,128)(2,1)} %all-gather.7.cloned.1.call-done, bf16[128,2048]{1,0:T(8,128)(2,1)S(1)} %bitcast.222), kind=kOutput, calls=%fused_computation.4 | convolution fusion | flops 1074397184 | bytes 9437184 | tf_op jit(solution)/shard_map/dot_general | solution.py:220
  274.7 21.8 %all_to_all.17 = bf16[8,16,2048]{2,1,0:T(8,128)(2,1)S(1)} all-to-all(bf16[8,16,2048]{2,1,0:T(8,128)(2,1)S(1)} %bitcast.223), channel_id=1, replica_groups=mesh['sp_0'=16,'sp_1'=4,'tp'=8] {'tp'}, dimensions={0} | all-to-all | bytes 1048576 | tf_op jit(solution)/shard_map/all_to_all | solution.py:70
  296.5 0.7 fusion.116
  (40 shorter events, 2.2 us)
Async XLA Ops:
  6.5 108.4 %copy-start = (bf16[512,2048]{1,0:T(8,128)(2,1)S(1)}, bf16[512,2048]{1,0:T(8,128)(2,1)}, u32[]{:S(2)}) copy-start(bf16[512,2048]{1,0:T(8,128)(2,1)} %param.30) | copy-start | bytes 6291460
  6.5 105.3 %all-gather.5.cloned.1.call-start = ((), (), s32[]{:S(2)}) async-start(), calls=%async_computation.3 | async-start | bytes 2228224 | tf_op jit(solution)/shard_map/all_gather | solution.py:47
  7.6 21.8 %collective-permute-start.2 = (bf16[3,512]{0,1:T(8,128)(2,1)S(1)}, bf16[3,512]{0,1:T(8,128)(2,1)S(1)}, u32[]{:S(2)}, u32[]{:S(2)}) collective-permute-start(bf16[3,512]{0,1:T(8,128)(2,1)S(1)} %copy.24), channel_id=1, source_target_pairs={{0,8},{8,16},{16,24},{24,32},{32,40},{40,48},{48,56},{56,64},{64,7... | collective-permute-start | bytes 9224 | tf_op jit(solution)/shard_map/ppermute | solution.py:32
  12.3 16.0 %collective-permute-start.1 = (bf16[3,128]{1,0:T(4,128)(2,1)S(1)}, bf16[3,128]{1,0:T(4,128)(2,1)S(1)}, u32[]{:S(2)}, u32[]{:S(2)}) collective-permute-start(bf16[3,128]{1,0:T(4,128)(2,1)S(1)} %slice.204), channel_id=1, source_target_pairs={{0,8},{8,16},{16,24},{24,32},{32,40},{40,48},{48,56},{56,64},{64,7... | collective-permute-start | bytes 2312 | tf_op jit(solution)/shard_map/ppermute | solution.py:32
  42.3 226.8 %all-gather.7.cloned.1.call-start = ((), (), s32[]{:S(2)}) async-start(), calls=%async_computation.4 | async-start | bytes 8519680 | tf_op jit(solution)/shard_map/all_gather | solution.py:19
  44.6 31.1 %collective-permute-start = (bf16[3,128]{1,0:T(4,128)(2,1)S(1)}, bf16[3,128]{1,0:T(4,128)(2,1)S(1)}, u32[]{:S(2)}, u32[]{:S(2)}) collective-permute-start(bf16[3,128]{1,0:T(4,128)(2,1)S(1)} %slice.196), channel_id=1, source_target_pairs={{0,8},{8,16},{16,24},{24,32},{32,40},{40,48},{48,56},{56,64},{64,7... | collective-permute-start | bytes 2312 | tf_op jit(solution)/shard_map/ppermute | solution.py:32
  111.8 3.1 %copy-start.3 = (f32[512]{0:T(512)S(1)}, f32[512]{0:T(512)}, u32[]{:S(2)}) copy-start(f32[512]{0:T(512)} %param.29) | copy-start | bytes 6148
  114.3 24.5 %copy-start.1 = (bf16[16,2048]{1,0:T(8,128)(2,1)S(1)}, bf16[16,2048]{1,0:T(8,128)(2,1)}, u32[]{:S(2)}) copy-start(bf16[16,2048]{1,0:T(8,128)(2,1)} %param.17) | copy-start | bytes 196612
  114.3 24.7 %copy-start.2 = (f32[2048]{0:T(1024)S(1)}, f32[2048]{0:T(1024)}, u32[]{:S(2)}) copy-start(f32[2048]{0:T(1024)} %param.31) | copy-start | bytes 24580
Sparse Core Ops, SparseCore 0:
  42.4 69.3 all-gather.4
  114.8 154.2 all-gather.6
where the time goes:
time: 305 us; the launch traced here: 304 us
  waiting for transfers between devices  152 us (50%)
  blocking collectives  104 us (34%)
  between operations  13.7 us (4%)
  other arithmetic  10.1 us (3%)
  matrix products  9.51 us (3%)
  starting transfers between devices  8.53 us (3%)
  local copies, waits for them, and re-layouts  6.08 us (2%)
    all_gather x1, waiting for transfers between devices, turned_gather(): out = lax.all_gather(both, axis, axis=0, tiled=True)  117 us
    all_gather x3, blocking collectives, entering_2(): lax.all_gather(part.astype(kind), axis)  46.3 us
    all_to_all x2, blocking collectives, sum_at_owner(): lax.all_to_all(blocks, axis, split_axis=0, concat_axis=0, tiled=True)  45.1 us
    all_gather x1, waiting for transfers between devices, entering_2(): lax.all_gather(part.astype(kind), axis)  34.8 us
    all_to_all x1, blocking collectives, copy_for_each(): return lax.all_to_all(copies, axis, split_axis=0, concat_axis=0, tiled=True)  12.8 us
    ppermute x3, starting transfers between devices, shifted(): lax.ppermute(value, axis, [(source, source + steps) for source in range(i...  8.49 us
  transfers between devices with their start and end apart: 5, of which 2 were waited for; matrix products, arithmetic and copies ran while one was open for 6% of the time, Pallas kernels for 0%

commit v1 on v0

--- a/solution.py
+++ b/solution.py
@@ -16,7 +16,9 @@
     turned = [jnp.moveaxis(a, dim, 0) for a, dim in zip(arrays, dims)]
     widths = [t[0].size for t in turned]
     both = jnp.concatenate([t.reshape(-1, w) for t, w in zip(turned, widths)], axis=1)
-    out = lax.all_gather(both, axis, axis=0, tiled=True)
+    out = jnp.concatenate(
+        lax.all_to_all(jnp.stack([both] * lax.axis_size(axis)), axis, 0, 0), axis=0
+    )
     blocks = jnp.split(out, [sum(widths[:k]) for k in range(1, len(widths))], axis=1)
     return tuple(
         (

time: 305 us -> 562 us (1.84)
  blocking collectives: 104 us -> 463 us
  waiting for transfers between devices: 152 us -> 46.3 us
    all_to_all x1, blocking collectives: 12.8 us -> 376 us  [turned_gather(): lax.all_to_all(jnp.stack([both] * lax.axis_size(axis)), axis, 0, 0)]
    all_gather x1 -> x0, waiting for transfers between devices: 117 us -> none  [turned_gather(): out = lax.all_gather(both, axis, axis=0, tiled=True)]
    all_to_all x0 -> x1, waiting for transfers between devices: none -> 9.35 us  [copy_for_each(): return lax.all_to_all(copies, axis, split_axis=0, concat_axis=0, tiled=True)]
  transfers between devices with their start and end apart: 5 -> 5, of which waited for: 2 -> 2; matrix products, arithmetic and copies ran while one was open for 6% -> 2% of each run, Pallas kernels for 0% -> 0%
where the time goes in v1:
time: 562 us
  blocking collectives  463 us (82%)
  waiting for transfers between devices  46.3 us (8%)
  between operations  13.7 us (2%)
  starting transfers between devices  12.9 us (2%)
  matrix products  9.48 us (2%)
  other arithmetic  8.51 us (2%)
  local copies, waits for them, and re-layouts  7.94 us (1%)
    all_to_all x1, blocking collectives, turned_gather(): lax.all_to_all(jnp.stack([both] * lax.axis_size(axis)), axis, 0, 0)  376 us
    all_gather x3, blocking collectives, entering_2(): lax.all_gather(part.astype(kind), axis)  46.1 us
    all_to_all x2, blocking collectives, sum_at_owner(): lax.all_to_all(blocks, axis, split_axis=0, concat_axis=0, tiled=True)  41.2 us
    all_gather x1, waiting for transfers between devices, entering_2(): lax.all_gather(part.astype(kind), axis)  36.9 us
  transfers between devices with their start and end apart: 5, of which 2 were waited for; matrix products, arithmetic and copies ran while one was open for 2% of the time, Pallas kernels for 0%

profile of v1, /device:TPU:1, one launch (start us, length us, event | category | flops | bytes accessed | tf_op | source)
XLA Modules:
  0.0 561.6 jit_solution(11087689786327529356)
XLA Ops:
  6.5 0.9 slice.212
  7.6 4.0 collective-permute-start.2
  11.6 0.7 slice.204
  12.3 3.2 collective-permute-start.1
  15.5 0.7 exp.73
  16.2 0.8 fusion.190
  17.5 0.8 slice_convert_fusion.3
  18.4 8.0 %all-gather = bf16[4,1,8,1]{2,3,1,0:T(2,128)(2,1)S(1)} all-gather(bf16[1,1,8,1]{2,3,1,0:T(2,128)(2,1)S(1)} %copy.27), channel_id=2, replica_groups=mesh['sp_0'=16,'sp_1'=4,'tp'=8] {'sp_1'}, dimensions={0}, use_global_device_ids=true | all-gather | bytes 80 | tf_op jit(solution)/shard_map/all_gather | solution.py:49
  26.4 0.8 bitcast_convert_fusion.3
  27.3 1.0 copy.25
  28.3 1.0 divide_multiply_fusion.1
  30.0 11.4 %all-gather.1 = bf16[32,64,128]{2,1,0:T(8,128)(2,1)S(1)} all-gather(bf16[8,64,128]{2,1,0:T(8,128)(2,1)S(1)} %fusion.22), channel_id=3, replica_groups=mesh['sp_0'=16,'sp_1'=4,'tp'=8] {'sp_1'}, dimensions={0}, use_global_device_ids=true | all-gather | bytes 655360 | tf_op jit(solution)/shard_map/all_gather | solution.py:49
  41.4 0.8 fusion.104
  42.3 0.7 slice.196
  43.0 1.3 collective-permute-start
  44.3 1.0 copy.28
  45.3 0.7 broadcast_in_dim.20
  46.1 26.8 %all_gather.19 = bf16[16,1,8]{2,1,0:T(2,128)(2,1)S(1)} all-gather(bf16[1,1,8]{2,1,0:T(2,128)(2,1)S(1)} %convert_bitcast_fusion), channel_id=1, replica_groups=mesh['sp_0'=16,'sp_1'=4,'tp'=8] {'sp_0'}, dimensions={0}, use_global_device_ids=true | all-gather | bytes 272 | tf_op jit(solution)/shard_map/all_gather | solution.py:49
  72.9 0.8 bitcast_convert_fusion.7
  73.8 1.0 divide_multiply_fusion.2
  75.1 36.9 %all-gather.4.cloned.1.call-done = bf16[16,1,8,64,128]{4,3,2,1,0:T(8,128)(2,1)} async-done(((bf16[1,1,8,64,128]{4,3,2,1,0:T(8,128)(2,1)}), bf16[16,1,8,64,128]{4,3,2,1,0:T(8,128)(2,1)}) %all-gather.4.cloned.1.call-update) | async-done | bytes 2097168 | tf_op jit(solution)/shard_map/all_gather | solution.py:49
  112.0 2.5 fusion.18
  115.1 0.6 convolution_convert_fusion
  115.7 23.0 %all_to_all.20 = bf16[8,16,2048]{2,1,0:T(8,128)(2,1)S(1)} all-to-all(bf16[8,16,2048]{2,1,0:T(8,128)(2,1)S(1)} %bitcast.223), channel_id=1, replica_groups=mesh['sp_0'=16,'sp_1'=4,'tp'=8] {'tp'}, dimensions={0} | all-to-all | bytes 1048576 | tf_op jit(solution)/shard_map/all_to_all | solution.py:72
  139.0 0.8 broadcast_in_dim.21
  139.9 4.4 all-to-all-start.1
  144.3 9.4 %all-to-all-done.1 = bf16[8,16,2048]{2,1,0:T(8,128)(2,1)S(1)} async-done(((bf16[8,16,2048]{2,1,0:T(8,128)(2,1)}), bf16[8,16,2048]{2,1,0:T(8,128)(2,1)S(1)}, u32[]{:S(2)}, u32[]{:S(2)}) %all-to-all-start.1) | async-done | bytes 524320 | tf_op jit(solution)/shard_map/all_to_all | solution.py:78
  153.7 1.1 stack.2
  154.7 375.5 %all_to_all.21 = bf16[64,32,2048]{2,1,0:T(8,128)(2,1)} all-to-all(bf16[64,32,2048]{2,1,0:T(8,128)(2,1)S(1)} %stack.2), channel_id=1, replica_groups=mesh['sp_0'=16,'sp_1'=4,'tp'=8] {'sp_0','sp_1'}, dimensions={0} | all-to-all | bytes 16777216 | tf_op jit(solution)/shard_map/all_to_all | solution.py:20
  530.3 5.6 fusion.4
  535.8 18.2 %all_to_all.22 = bf16[8,16,2048]{2,1,0:T(8,128)(2,1)S(1)} all-to-all(bf16[8,16,2048]{2,1,0:T(8,128)(2,1)S(1)} %bitcast.225), channel_id=1, replica_groups=mesh['sp_0'=16,'sp_1'=4,'tp'=8] {'tp'}, dimensions={0} | all-to-all | bytes 1048576 | tf_op jit(solution)/shard_map/all_to_all | solution.py:72
  554.1 0.7 fusion.116
  (44 shorter events, 3.0 us)
Async XLA Ops:
  6.5 108.6 %copy-start = (bf16[512,2048]{1,0:T(8,128)(2,1)S(1)}, bf16[512,2048]{1,0:T(8,128)(2,1)}, u32[]{:S(2)}) copy-start(bf16[512,2048]{1,0:T(8,128)(2,1)} %param.30) | copy-start | bytes 6291460
  6.5 105.5 %all-gather.4.cloned.1.call-start = ((), (), s32[]{:S(2)}) async-start(), calls=%async_computation.4 | async-start | bytes 2228224 | tf_op jit(solution)/shard_map/all_gather | solution.py:49
  7.6 21.8 %collective-permute-start.2 = (bf16[3,512]{0,1:T(8,128)(2,1)S(1)}, bf16[3,512]{0,1:T(8,128)(2,1)S(1)}, u32[]{:S(2)}, u32[]{:S(2)}) collective-permute-start(bf16[3,512]{0,1:T(8,128)(2,1)S(1)} %copy.24), channel_id=1, source_target_pairs={{0,8},{8,16},{16,24},{24,32},{32,40},{40,48},{48,56},{56,64},{64,7... | collective-permute-start | bytes 9224 | tf_op jit(solution)/shard_map/ppermute | solution.py:34
  12.3 16.0 %collective-permute-start.1 = (bf16[3,128]{1,0:T(4,128)(2,1)S(1)}, bf16[3,128]{1,0:T(4,128)(2,1)S(1)}, u32[]{:S(2)}, u32[]{:S(2)}) collective-permute-start(bf16[3,128]{1,0:T(4,128)(2,1)S(1)} %slice.204), channel_id=1, source_target_pairs={{0,8},{8,16},{16,24},{24,32},{32,40},{40,48},{48,56},{56,64},{64,7... | collective-permute-start | bytes 2312 | tf_op jit(solution)/shard_map/ppermute | solution.py:34
  43.0 30.8 %collective-permute-start = (bf16[3,128]{1,0:T(4,128)(2,1)S(1)}, bf16[3,128]{1,0:T(4,128)(2,1)S(1)}, u32[]{:S(2)}, u32[]{:S(2)}) collective-permute-start(bf16[3,128]{1,0:T(4,128)(2,1)S(1)} %slice.196), channel_id=1, source_target_pairs={{0,8},{8,16},{16,24},{24,32},{32,40},{40,48},{48,56},{56,64},{64,7... | collective-permute-start | bytes 2312 | tf_op jit(solution)/shard_map/ppermute | solution.py:34
  112.0 3.1 copy-start.5
  114.5 24.2 %copy-start.1 = (bf16[16,2048]{1,0:T(8,128)(2,1)S(1)}, bf16[16,2048]{1,0:T(8,128)(2,1)}, u32[]{:S(2)}) copy-start(bf16[16,2048]{1,0:T(8,128)(2,1)} %param.17) | copy-start | bytes 196612
  114.5 24.4 %copy-start.4 = (f32[2048]{0:T(1024)S(1)}, f32[2048]{0:T(1024)}, u32[]{:S(2)}) copy-start(f32[2048]{0:T(1024)} %param.31) | copy-start | bytes 24580
  114.5 29.7 %copy-start.2 = (bf16[1024,32]{0,1:T(8,128)(2,1)S(1)}, bf16[1024,32]{0,1:T(8,128)(2,1)}, u32[]{:S(2)}) copy-start(bf16[1024,32]{0,1:T(8,128)(2,1)} %param.33) | copy-start | bytes 196612
  114.6 29.7 %copy-start.3 = (bf16[32,1024]{1,0:T(8,128)(2,1)S(1)}, bf16[32,1024]{1,0:T(8,128)(2,1)}, u32[]{:S(2)}) copy-start(bf16[32,1024]{1,0:T(8,128)(2,1)} %param.32) | copy-start | bytes 196612
  139.9 13.8 %all-to-all-start.1 = ((bf16[8,16,2048]{2,1,0:T(8,128)(2,1)}), bf16[8,16,2048]{2,1,0:T(8,128)(2,1)S(1)}, u32[]{:S(2)}, u32[]{:S(2)}) async-start(bf16[8,16,2048]{2,1,0:T(8,128)(2,1)} %broadcast_in_dim.21), calls=%async_computation.1 | async-start | bytes 1048576 | tf_op jit(solution)/shard_map/all_to_all | solution.py:78
Sparse Core Ops, SparseCore 0:
  42.4 69.5 all-gather.3
